TPU v7x, 32 devices: a whole 2x2x4 slice. The times are simulated.
32 devices in a mesh: sp: 8 (over z, x), tp: 4 (over y, core).
Axes of the slice: x: 2, y: 2, z: 4, core: 2. Of those that a mesh axis runs over, the one named last changes fastest.
Arguments:
- tokens: bfloat16 [4096, 2048], P('sp', 'tp'), may hold values from -72 to 72
- w_query: bfloat16 [2048, 1024], P('sp', 'tp'), may hold values from -0.125 to 0.125
- w_key: bfloat16 [2048, 256], P('sp', 'tp'), may hold values from -0.125 to 0.125
- w_value: bfloat16 [2048, 256], P('sp', 'tp'), may hold values from -0.125 to 0.125
- w_pool_in: bfloat16 [2048, 1024], P('sp', 'tp'), may hold values from -0.125 to 0.125
- sink: float32 [16], P('tp'), may hold values from 3 to 7
- w_pool: bfloat16 [4, 256, 256], P('tp'), may hold values from -0.375 to 0.375
- pool_scale: float32 [1024], P('tp'), may hold values from 0.1 to 1.9
- w_out_attn: bfloat16 [1024, 2048], P('tp', 'sp'), may hold values from -0.5 to 0.5
- w_out_pool: bfloat16 [1024, 2048], P('tp', 'sp'), may hold values from -0.125 to 0.125
- out_gain: float32 [2048], P('tp'), may hold values from 0.1 to 1.9
Outputs:
- mixed: bfloat16 [4096, 2048], P('sp', 'tp')
All inputs are finite; a program needn't handle non-finite values.
Results may differ from a plain program's by a relative error of at most 0.012.
The roundings to bfloat16 on the way count: a program that leaves them out, or rounds other values in their place, can miss the bound.
Values may be sent and summed in bfloat16 or wider, within the bound.
A program may use at most 64 MiB of HBM per device.

v0:
```python
import jax
import jax.numpy as jnp
from jax import lax
from jax.sharding import PartitionSpec as P

HEAD_DIM = 64
POOL_GROUPS = 4
WINDOW = 128


epsilon = 1e-05
masked_score = -1e30


def padded(cells, sides, width):
    for axis, dim in sides:
        count = lax.axis_size(axis)
        ends = count - 1
        head = lax.slice_in_dim(cells, 0, width, axis=dim)
        tail = lax.slice_in_dim(cells, cells.shape[dim] - width, cells.shape[dim], axis=dim)
        cells = jnp.concatenate(
            [
                lax.ppermute(tail, axis, [(i, (i + 1) % count) for i in range(ends)]),
                cells,
                lax.ppermute(head, axis, [((i + 1) % count, i) for i in range(ends)]),
            ],
            axis=dim,
        )
    return cells


def make_projector(gathered, pieces):
    piece_query, piece_key, piece_value, piece_chan = pieces
    joined = jnp.concatenate([piece_key, piece_value], axis=1)
    return (
        jnp.dot(gathered, piece_query, preferred_element_type=jnp.float32),
        jnp.dot(gathered, joined, preferred_element_type=jnp.float32),
        jnp.dot(gathered, piece_chan, preferred_element_type=jnp.float32),
    )


def attend_local(query, keys_ext, sinks, offset, seq_len, key_cols):
    tok_rows, query_cols = query.shape
    kv_local = key_cols // HEAD_DIM
    group = query_cols // key_cols
    block_count = tok_rows // WINDOW
    stacked = keys_ext.reshape(block_count + 2, WINDOW, 2 * key_cols)
    banded = jnp.concatenate([stacked[:-2], stacked[1:-1], stacked[2:]], axis=1)
    key_band = banded[:, :, :key_cols].reshape(block_count, 3 * WINDOW, kv_local, HEAD_DIM)
    value_band = banded[:, :, key_cols:].reshape(block_count, 3 * WINDOW, kv_local, HEAD_DIM)
    query_blocks = query.reshape(block_count, WINDOW, kv_local, group, HEAD_DIM)
    scores = jnp.einsum(
        "nqkgd,nskd->nkgqs", query_blocks, key_band, preferred_element_type=jnp.float32
    ) * HEAD_DIM ** (-0.5)
    starts = offset + jnp.arange(block_count, dtype=jnp.int32) * WINDOW
    query_pos = starts[:, None] + jnp.arange(WINDOW, dtype=jnp.int32)[None, :]
    key_pos = starts[:, None] + jnp.arange(3 * WINDOW, dtype=jnp.int32)[None, :] - WINDOW
    distance = key_pos[:, None, :] - query_pos[:, :, None]
    inside = (key_pos >= 0) & (key_pos < seq_len)
    keep = (jnp.abs(distance) <= WINDOW) & inside[:, None, :]
    scores = jnp.where(keep[:, None, None], scores, masked_score)
    sink_logit = sinks.reshape(kv_local, group)[None, :, :, None, None]
    top = jnp.maximum(jnp.max(scores, axis=-1, keepdims=True), sink_logit)
    raised = jnp.exp(scores - top)
    total = jnp.sum(raised, axis=-1, keepdims=True) + jnp.exp(sink_logit - top)
    probs = (raised / total).astype(jnp.bfloat16)
    attended = jnp.einsum(
        "nkgqs,nskd->nqkgd", probs, value_band, preferred_element_type=jnp.float32
    )
    return attended.astype(jnp.bfloat16).reshape(tok_rows, query_cols)


def local(
    tokens,
    w_query,
    w_key,
    w_value,
    w_pool_in,
    sink,
    w_pool,
    pool_scale,
    w_out_attn,
    w_out_pool,
    out_gain,
):
    tok_rows = tokens.shape[0]
    seq_len = tok_rows * lax.axis_size("sp")
    offset = lax.axis_index("sp") * tok_rows
    out_both = jnp.concatenate([w_out_attn, w_out_pool], axis=0)
    gathered = lax.all_gather(tokens, "tp", axis=1, tiled=True)
    key_cols = w_key.shape[1]
    chan_cols = w_pool_in.shape[1]
    query_sum, joined_sum, chan_sum = make_projector(
        gathered,
        (
            lax.all_gather(w_query, "sp", axis=0, tiled=True),
            lax.all_gather(w_key, "sp", axis=0, tiled=True),
            lax.all_gather(w_value, "sp", axis=0, tiled=True),
            lax.all_gather(w_pool_in, "sp", axis=0, tiled=True),
        ),
    )
    query = query_sum.astype(jnp.bfloat16)
    key_value = joined_sum.astype(jnp.bfloat16)
    chan = chan_sum.astype(jnp.bfloat16)
    keys_ext = padded(key_value, (("sp", 0),), WINDOW)
    attended = attend_local(query, keys_ext, sink, offset, seq_len, key_cols)
    rim_rows = 2 ** (POOL_GROUPS - 1)
    chan_ext = padded(chan, (("sp", 0),), rim_rows)
    running = jnp.concatenate(
        [jnp.zeros((1, chan_cols), jnp.float32), jnp.cumsum(chan_ext.astype(jnp.float32), axis=0)],
        axis=0,
    )
    chan_float = chan.astype(jnp.float32)
    positions = offset + jnp.arange(tok_rows, dtype=jnp.int32)
    group_count = w_pool.shape[0]
    level = lax.axis_index("tp") * group_count + 0
    half = jnp.left_shift(jnp.int32(1), level)
    upper = lax.dynamic_slice_in_dim(running, rim_rows + half, tok_rows, 0)
    lower = lax.dynamic_slice_in_dim(running, rim_rows - half, tok_rows, 0)
    count = (
        jnp.clip(positions + half, 0, seq_len) - jnp.clip(positions - half, 0, seq_len)
    ).astype(jnp.float32)
    spread = ((upper - lower) / count[:, None] - chan_float).astype(jnp.bfloat16)
    outputs = jnp.dot(spread, w_pool[0], preferred_element_type=jnp.float32)
    pooled = (outputs * pool_scale).astype(jnp.bfloat16)
    hidden = jnp.concatenate([attended, pooled], axis=1)
    terms = jnp.dot(
        hidden,
        lax.all_gather(out_both, "sp", axis=1, tiled=True),
        preferred_element_type=jnp.float32,
    )
    share_width = out_gain.shape[0]
    model_width = share_width * lax.axis_size("tp")
    share = lax.psum_scatter(
        terms.astype(jnp.bfloat16), "tp", scatter_dimension=1, tiled=True
    ).astype(jnp.float32)
    row_total, row_square = lax.psum((jnp.sum(share, axis=1), jnp.sum(share * share, axis=1)), "tp")
    row_mean = row_total / model_width
    variance = row_square / model_width - row_mean * row_mean
    normed = (share - row_mean[:, None]) * lax.rsqrt(variance + epsilon)[:, None] * out_gain
    return normed.astype(jnp.bfloat16)


def solution(mesh):
    return jax.shard_map(
        local,
        mesh=mesh,
        in_specs=(
            P("sp", "tp"),
            P("sp", "tp"),
            P("sp", "tp"),
            P("sp", "tp"),
            P("sp", "tp"),
            P("tp"),
            P("tp", None, None),
            P("tp"),
            P("tp", "sp"),
            P("tp", "sp"),
            P("tp"),
        ),
        out_specs=P("sp", "tp"),
        check_vma=False,
    )
```

profile of v0, /device:TPU:0, one launch (start us, length us, event | category | flops | bytes accessed | tf_op | source)
XLA Modules:
  0.0 219.0 jit_solution(90208195681384084)
XLA Ops:
  6.5 0.7 all-gather.5.cloned.1.call-update
  7.3 0.7 all-gather.9.cloned.1.call-update
  8.1 0.7 all-gather.7.cloned.1.call-update
  8.8 1.7 pad_maximum_fusion
  10.7 0.1 compare_and_fusion
  10.8 32.8 %all_gather.18 = bf16[2048,64]{0,1:T(8,128)(2,1)S(1)} all-gather(bf16[256,64]{0,1:T(8,128)(2,1)} %param.13), channel_id=1, replica_groups=mesh['sp'=8,'tp'=4] {'sp'}, dimensions={0}, use_global_device_ids=true | all-gather | bytes 294912 | tf_op jit(solution)/shard_map/all_gather | solution.py:97
  43.6 31.3 %all_gather.19 = bf16[2048,64]{0,1:T(8,128)(2,1)S(1)} all-gather(bf16[256,64]{0,1:T(8,128)(2,1)} %param.14), channel_id=1, replica_groups=mesh['sp'=8,'tp'=4] {'sp'}, dimensions={0}, use_global_device_ids=true | all-gather | bytes 294912 | tf_op jit(solution)/shard_map/all_gather | solution.py:98
  74.9 0.6 fusion.17
  75.5 2.4 %convolution_convert_fusion.3 = bf16[128,512]{1,0:T(8,128)(2,1)S(1)} fusion(bf16[512,2048]{1,0:T(8,128)(2,1)} %all-gather.5.cloned.1.call-done, bf16[2048,64]{0,1:T(8,128)(2,1)S(1)} %all_gather.19, bf16[2048,64]{0,1:T(8,128)(2,1)S(1)} %all_gather.18), kind=kOutput, calls=%fused_computation.17 | convolution fusion | flops 269549568 | bytes 2752512 | tf_op jit(solution)/shard_map/dot_general | solution.py:37
  78.0 3.4 %collective-permute-start = (bf16[128,128]{0,1:T(8,128)(2,1)S(1)}, bf16[128,128]{0,1:T(8,128)(2,1)S(1)}, u32[]{:S(2)}, u32[]{:S(2)}) collective-permute-start(bf16[128,128]{0,1:T(8,128)(2,1)S(1)} %get-tuple-element.14), channel_id=1, source_target_pairs={{0,4},{4,8},{8,12},{12,16},{16,20},{20,24},{24,28},{1,5},{5,9},{9,... | collective-permute-start | bytes 98312 | tf_op jit(solution)/shard_map/ppermute | solution.py:23
  81.4 1.3 collective-permute-start.1
  82.8 2.6 %convolution_convert_fusion.1 = bf16[512,256]{1,0:T(8,128)(2,1)S(1)} fusion(bf16[512,2048]{1,0:T(8,128)(2,1)} %all-gather.5.cloned.1.call-done, bf16[2048,256]{1,0:T(8,128)(2,1)} %all-gather.9.cloned.1.call-done), kind=kOutput, calls=%fused_computation.12 | convolution fusion | flops 537001984 | bytes 3407872 | tf_op jit(solution)/shard_map/dot_general | solution.py:38
  85.3 4.6 %collective-permute-start.2 = (bf16[8,256]{1,0:T(8,128)(2,1)S(1)}, bf16[8,256]{1,0:T(8,128)(2,1)S(1)}, u32[]{:S(2)}, u32[]{:S(2)}) collective-permute-start(bf16[8,256]{1,0:T(8,128)(2,1)S(1)} %get-tuple-element.9), channel_id=1, source_target_pairs={{0,4},{4,8},{8,12},{12,16},{16,20},{20,24},{24,28},{1,5},{5,9},{9,... | collective-permute-start | bytes 12296 | tf_op jit(solution)/shard_map/ppermute | solution.py:23
  89.9 1.3 collective-permute-start.3
  91.2 27.4 %all-gather.7.cloned.1.call-done = bf16[2048,256]{1,0:T(8,128)(2,1)} async-done(((bf16[256,256]{1,0:T(8,128)(2,1)}), bf16[2048,256]{1,0:T(8,128)(2,1)}) %all-gather.7.cloned.1.call-update) | async-done | bytes 1048592 | tf_op jit(solution)/shard_map/all_gather | solution.py:96
  118.6 2.6 %convolution_convert_fusion.2 = bf16[512,256]{1,0:T(8,128)(2,1)S(1)} fusion(bf16[512,2048]{1,0:T(8,128)(2,1)} %all-gather.5.cloned.1.call-done, bf16[2048,256]{1,0:T(8,128)(2,1)} %all-gather.7.cloned.1.call-done), kind=kOutput, calls=%fused_computation.13 | convolution fusion | flops 537001984 | bytes 3407872 | tf_op jit(solution)/shard_map/dot_general | solution.py:36
  121.2 0.2 reshape.154
  121.6 0.7 fusion.15
  122.3 0.1 broadcast_add_fusion
  122.3 0.2 copy.27
  122.6 0.4 fusion.4
  123.3 0.7 fusion.1
  124.1 0.7 fusion
  124.8 0.1 exponential_add_fusion
  124.8 1.0 fusion.8
  125.8 0.2 copy.25
  126.0 43.5 %all-gather.11.cloned.1.call-done = bf16[512,2048]{1,0:T(8,128)(2,1)} async-done(((bf16[512,256]{1,0:T(8,128)(2,1)}), bf16[512,2048]{1,0:T(8,128)(2,1)}) %all-gather.11.cloned.1.call-update) | async-done | bytes 2097168 | tf_op jit(solution)/shard_map/all_gather | solution.py:129
  169.6 4.3 %convolution_convert_fusion = bf16[512,2048]{1,0:T(8,128)(2,1)} fusion(bf16[512,2048]{1,0:T(8,128)(2,1)} %all-gather.11.cloned.1.call-done, bf16[512,256]{0,1:T(8,128)(2,1)S(1)} %fusion.4, bf16[512,256]{0,1:T(8,128)(2,1)S(1)} %bitcast.85), kind=kOutput, calls=%fused_computation.3 | convolution fusion | flops 1075838976 | bytes 4718592 | tf_op jit(solution)/shard_map/dot_general | solution.py:127
  173.9 29.5 %reduce-scatter.2.cloned.1.call-done = bf16[512,512]{1,0:T(8,128)(2,1)} async-done(((bf16[512,2048]{1,0:T(8,128)(2,1)}), bf16[512,512]{1,0:T(8,128)(2,1)}) %reduce-scatter.2.cloned.1.call-update) | async-done | bytes 524304 | tf_op jit(solution)/shard_map/reduce_scatter | solution.py:134
  203.4 1.3 convert_reduce_fusion
  204.7 5.8 %all-reduce.2 = (f32[512]{0:T(512)S(1)}, f32[512]{0:T(512)S(1)}) all-reduce(f32[512]{0:T(512)S(1)} %get-tuple-element.6, f32[512]{0:T(512)S(1)} %get-tuple-element.5), channel_id=1, replica_groups=mesh['sp'=8,'tp'=4] {'tp'}, use_global_device_ids=true, to_apply=%region_8.9 | all-reduce | flops 1024 | bytes 8192 | tf_op jit(solution)/shard_map/psum | solution.py:137
  210.4 2.1 fusion.13
  (40 shorter events, 0.9 us)
Async XLA Ops:
  6.5 116.1 %copy-start = (bf16[1,256,256]{2,1,0:T(8,128)(2,1)S(1)}, bf16[1,256,256]{2,1,0:T(8,128)(2,1)}, u32[]{:S(2)}) copy-start(bf16[1,256,256]{2,1,0:T(8,128)(2,1)} %param.17) | copy-start | bytes 393220
  6.5 69.0 %all-gather.5.cloned.1.call-start = ((), (), s32[]{:S(2)}) async-start(), calls=%async_computation.1 | async-start | bytes 2621440 | tf_op jit(solution)/shard_map/all_gather | solution.py:90
  7.3 75.5 %all-gather.9.cloned.1.call-start = ((), (), s32[]{:S(2)}) async-start(), calls=%async_computation.3 | async-start | bytes 1179648 | tf_op jit(solution)/shard_map/all_gather | solution.py:99
  8.0 110.6 %all-gather.7.cloned.1.call-start = ((), (), s32[]{:S(2)}) async-start(), calls=%async_computation.2 | async-start | bytes 1179648 | tf_op jit(solution)/shard_map/all_gather | solution.py:96
  8.7 160.8 %all-gather.11.cloned.1.call-start = ((), (), s32[]{:S(2)}) async-start(), calls=%async_computation.4 | async-start | bytes 2359296 | tf_op jit(solution)/shard_map/all_gather | solution.py:129
  10.5 192.9 %reduce-scatter.2.cloned.1.call-start = ((), (), s32[]{:S(2)}) async-start(), calls=%async_computation.5 | async-start | bytes 2621440 | tf_op jit(solution)/shard_map/reduce_scatter | solution.py:134
  78.0 45.1 %collective-permute-start = (bf16[128,128]{0,1:T(8,128)(2,1)S(1)}, bf16[128,128]{0,1:T(8,128)(2,1)S(1)}, u32[]{:S(2)}, u32[]{:S(2)}) collective-permute-start(bf16[128,128]{0,1:T(8,128)(2,1)S(1)} %get-tuple-element.14), channel_id=1, source_target_pairs={{0,4},{4,8},{8,12},{12,16},{16,20},{20,24},{24,28},{1,5},{5,9},{9,... | collective-permute-start | bytes 98312 | tf_op jit(solution)/shard_map/ppermute | solution.py:23
  81.4 41.6 %collective-permute-start.1 = (bf16[128,128]{0,1:T(8,128)(2,1)S(1)}, bf16[128,128]{0,1:T(8,128)(2,1)S(1)}, u32[]{:S(2)}, u32[]{:S(2)}) collective-permute-start(bf16[128,128]{0,1:T(8,128)(2,1)S(1)} %get-tuple-element.13), channel_id=1, source_target_pairs={{4,0},{8,4},{12,8},{16,12},{20,16},{24,20},{28,24},{5,1},{9,5},{13... | collective-permute-start | bytes 98312 | tf_op jit(solution)/shard_map/ppermute | solution.py:25
  85.3 36.1 %collective-permute-start.2 = (bf16[8,256]{1,0:T(8,128)(2,1)S(1)}, bf16[8,256]{1,0:T(8,128)(2,1)S(1)}, u32[]{:S(2)}, u32[]{:S(2)}) collective-permute-start(bf16[8,256]{1,0:T(8,128)(2,1)S(1)} %get-tuple-element.9), channel_id=1, source_target_pairs={{0,4},{4,8},{8,12},{12,16},{16,20},{20,24},{24,28},{1,5},{5,9},{9,... | collective-permute-start | bytes 12296 | tf_op jit(solution)/shard_map/ppermute | solution.py:23
  89.9 31.5 %collective-permute-start.3 = (bf16[8,256]{1,0:T(8,128)(2,1)S(1)}, bf16[8,256]{1,0:T(8,128)(2,1)S(1)}, u32[]{:S(2)}, u32[]{:S(2)}) collective-permute-start(bf16[8,256]{1,0:T(8,128)(2,1)S(1)} %get-tuple-element.10), channel_id=1, source_target_pairs={{4,0},{8,4},{12,8},{16,12},{20,16},{24,20},{28,24},{5,1},{9,5},{13... | collective-permute-start | bytes 12296 | tf_op jit(solution)/shard_map/ppermute | solution.py:25
  121.5 1.1 copy-start.3
  123.1 0.9 copy-start.2
  169.6 40.8 %copy-start.1 = (f32[512]{0:T(512)S(1)}, f32[512]{0:T(512)}, u32[]{:S(2)}) copy-start(f32[512]{0:T(512)} %param.21) | copy-start | bytes 6148
Sparse Core Ops, SparseCore 0:
  8.9 25.2 all-gather.4
  36.3 40.5 all-gather.8
  79.1 39.4 all-gather.6
  120.5 49.0 all-gather.10
  174.0 29.3 reduce-scatter.1
where the time goes:
time: 219 us
  waiting for transfers between devices  103 us (47%)
  blocking collectives  69.9 us (32%)
  matrix products  13.9 us (6%)
  between operations  13.4 us (6%)
  starting transfers between devices  10.7 us (5%)
  other arithmetic  7.57 us (3%)
    all_gather x1, waiting for transfers between devices, local(): lax.all_gather(out_both, 'sp', axis=1, tiled=True)  43.5 us
    all_gather x1, blocking collectives, local(): lax.all_gather(w_key, 'sp', axis=0, tiled=True)  32.8 us
    all_gather x1, blocking collectives, local(): lax.all_gather(w_value, 'sp', axis=0, tiled=True)  31.3 us
    reduce_scatter x1, waiting for transfers between devices, local(): lax.psum_scatter(terms.astype(jnp.bfloat16), 'tp', scatter_dimension=1, t...  29.5 us
    all_gather x1, waiting for transfers between devices, local(): lax.all_gather(w_query, 'sp', axis=0, tiled=True)  27.4 us
    ppermute x2, starting transfers between devices, padded(): lax.ppermute(tail, axis, [(i, (i + 1) % count) for i in range(ends)])  8 us
    psum x1, blocking collectives, local(): lax.psum((jnp.sum(share, axis=1), jnp.sum(share * share, axis=1)), 'tp')  5.76 us
  transfers between devices with their start and end apart: 9, of which 3 were waited for; matrix products, arithmetic and copies ran while one was open for 7% of the time, Pallas kernels for 0%

commit v1 on v0

--- a/solution.py
+++ b/solution.py
@@ -1,6 +1,10 @@
+import functools
+
 import jax
 import jax.numpy as jnp
 from jax import lax
+from jax.experimental import pallas as pl
+from jax.experimental.pallas import tpu as pltpu
 from jax.sharding import PartitionSpec as P
 
 HEAD_DIM = 64
@@ -141,9 +145,408 @@
     return normed.astype(jnp.bfloat16)
 
 
+MESH = pl.DeviceIdType.MESH
+RIM = 16
+
+
+def mixer_kernel(
+    n,
+    tp,
+    tok_ref,
+    wq_ref,
+    wk_ref,
+    wv_ref,
+    wc_ref,
+    sink_ref,
+    wp_ref,
+    ps_ref,
+    woa_ref,
+    wop_ref,
+    gain_ref,
+    out_ref,
+    win,
+    wout,
+    tok,
+    acc,
+    query,
+    kv,
+    chan,
+    hidden,
+    part,
+    landed,
+    stats,
+    win_send,
+    win_recv,
+    wout_send,
+    wout_recv,
+    tok_send,
+    tok_recv,
+    rim_send,
+    rim_recv,
+    part_send,
+    part_recv,
+    stat_send,
+    stat_recv,
+):
+    f32, bf16 = jnp.float32, jnp.bfloat16
+    me, t = lax.axis_index("sp"), lax.axis_index("tp")
+    rows = tok_ref.shape[0]
+    seq_len = rows * n
+    half_n = n // 2
+    column = me % 2
+    pos = (me // 2) * (1 - column) + column * (n - 1 - me // 2)
+
+    def at(p):
+        p = lax.rem(p + n, n)
+        back = p // half_n
+        return (1 - back) * (2 * p) + back * (2 * (n - 1 - p) + 1)
+
+    ring = (at(pos + 1), at(pos - 1))
+    after, before = lax.rem(me + 1, n), lax.rem(me + n - 1, n)
+    mate = t + 1 - 2 * lax.rem(t, 2)
+    across = lax.rem(t + 2, tp)
+    per = n // tp
+
+    def rdma(src, dst, send, recv, sp, tpi):
+        return pltpu.make_async_remote_copy(
+            src_ref=src,
+            dst_ref=dst,
+            send_sem=send,
+            recv_sem=recv,
+            device_id={"sp": sp, "tp": tpi},
+            device_id_type=MESH,
+        )
+
+    qc, kc = wq_ref.shape[1], wk_ref.shape[1]
+    cc = wc_ref.shape[1]
+    depth = wq_ref.shape[0]
+    hd = depth // 2
+    for h in range(2):
+        r = slice(h * hd, (h + 1) * hd)
+        win[me, h, :, 0:qc] = wq_ref[r, :]
+        win[me, h, :, qc : qc + 2 * kc] = jnp.concatenate([wk_ref[r, :], wv_ref[r, :]], axis=1)
+        win[me, h, :, qc + 2 * kc :] = wc_ref[r, :]
+    for b in range(per):
+        tok[t * per + b] = tok_ref[:, b * depth : (b + 1) * depth]
+    wout[me, 0] = woa_ref[...]
+    wout[me, 1] = wop_ref[...]
+
+    barrier = pltpu.get_barrier_semaphore()
+    peers = [(s, t) for s in ring] + [(s, t) for s in (before, after)]
+    peers += [(me, lax.rem(t + i, tp)) for i in range(1, tp)]
+    for s, p in peers:
+        pl.semaphore_signal(barrier, inc=1, device_id={"sp": s, "tp": p}, device_id_type=MESH)
+    pl.semaphore_wait(barrier, len(peers))
+
+    def ring_copy(buf, send, recv, way, k, hop):
+        sign = -1 if way == 0 else 1
+        h = k % 2 if way == 0 else 1 - k % 2
+        slot = buf.at[at(pos + sign * (k // 2 + hop)), h]
+        return rdma(slot, slot, send.at[way, k], recv.at[way, k], ring[way], t)
+
+    def w_in(way, k, hop):
+        return ring_copy(win, win_send, win_recv, way, k, hop)
+
+    def w_out(way, k, hop):
+        return ring_copy(wout, wout_send, wout_recv, way, k, hop)
+
+    def tok_copy(owner, b, i, dst):
+        slot = tok.at[owner * per + b]
+        return rdma(slot, slot, tok_send.at[i], tok_recv.at[i], me, dst)
+
+    for b in range(per):
+        tok_copy(t, b, b, across).start()
+        for way in range(2):
+            if b < 2:
+                w_in(way, b, 0).start()
+    for b in range(per):
+        tok_copy(t, b, per + b, mate).start()
+
+    last = n - 2
+    origin = [at(pos)]
+    for d in range(1, half_n):
+        origin += [at(pos - d), at(pos + d)]
+    origin.append(at(pos + half_n))
+
+    def project(i, first=False):
+        o = origin[i]
+        w = win[o].reshape(depth, qc + 2 * kc + cc)
+        term = jnp.dot(tok[o], w, preferred_element_type=f32)
+        if first:
+            acc[...] = term
+        else:
+            acc[...] += term
+
+    def relay(copy, k, after_last):
+        for way in range(2):
+            copy(way, k, 1).wait_recv()
+            if k + 2 <= last:
+                copy(way, k + 2, 0).start()
+            elif after_last is not None:
+                after_last(way, k + 1 - last)
+
+    def start_out(way, k):
+        w_out(way, k, 0).start()
+
+    ready = 0
+    done_blocks = 0
+    tok_step = {1: 0, 3: 1}
+    tokens_here = False
+    for k in range(last + 1):
+        relay(w_in, k, start_out)
+        if k in tok_step:
+            b = tok_step[k]
+            tok_copy(across, b, b, across).wait_recv()
+            tok_copy(across, b, 2 * per + b, mate).start()
+        if k == 3:
+            for b in range(per):
+                tok_copy(mate, b, per + b, mate).wait_recv()
+                tok_copy(lax.rem(mate + 2, tp), b, 2 * per + b, mate).wait_recv()
+            tokens_here = True
+        ready = 1 + 2 * ((k + 1) // 2) if k < last else n
+        if tokens_here:
+            while done_blocks < ready and (k == last or done_blocks < 1 + 2 * ((k - 2) // 1)):
+                project(done_blocks, done_blocks == 0)
+                done_blocks += 1
+
+    query[...] = acc[:, 0:qc].astype(bf16)
+    kv[WINDOW : WINDOW + rows, :] = acc[:, qc : qc + 2 * kc].astype(bf16)
+    chan[RIM : RIM + rows, :] = acc[:, qc + 2 * kc :].astype(bf16)
+
+    def rim(buf, width, down, i):
+        if down:
+            return rdma(buf.at[pl.ds(rows, width)], buf.at[pl.ds(0, width)], rim_send.at[i], rim_recv.at[i], after, t)
+        return rdma(
+            buf.at[pl.ds(width, width)], buf.at[pl.ds(rows + width, width)], rim_send.at[i], rim_recv.at[i], before, t
+        )
+
+    rims = [rim(kv, WINDOW, True, 0), rim(kv, WINDOW, False, 1), rim(chan, RIM, True, 2), rim(chan, RIM, False, 3)]
+    for c in rims:
+        c.start()
+
+    group = qc // kc
+
+    def attend(b):
+        band = kv[b * WINDOW : (b + 3) * WINDOW, :]
+        q = query[b * WINDOW : (b + 1) * WINDOW, :]
+        stacked = jnp.concatenate([q[:, g * HEAD_DIM : (g + 1) * HEAD_DIM] for g in range(group)], axis=0)
+        scores = lax.dot_general(
+            stacked, band[:, :HEAD_DIM], (((1,), (1,)), ((), ())), preferred_element_type=f32
+        ) * HEAD_DIM ** (-0.5)
+        scores = scores.reshape(group, WINDOW, 3 * WINDOW)
+        r = lax.broadcasted_iota(jnp.int32, (WINDOW, 3 * WINDOW), 0)
+        c = lax.broadcasted_iota(jnp.int32, (WINDOW, 3 * WINDOW), 1)
+        keep = (c >= r) & (c <= r + 2 * WINDOW)
+        key_pos = c + (me * rows + b * WINDOW - WINDOW)
+        keep = keep & (key_pos >= 0) & (key_pos < seq_len)
+        outs = []
+        for g in range(group):
+            s = jnp.where(keep, scores[g], masked_score)
+            logit = sink_ref[0, g]
+            top = jnp.maximum(jnp.max(s, axis=1, keepdims=True), logit)
+            raised = jnp.exp(s - top)
+            total = jnp.sum(raised, axis=1, keepdims=True) + jnp.exp(logit - top)
+            outs.append((raised * (1.0 / total)).astype(bf16))
+        got = jnp.dot(jnp.concatenate(outs, axis=0), band, preferred_element_type=f32)
+        got = got[:, HEAD_DIM : 2 * HEAD_DIM].astype(bf16)
+        hidden[b * WINDOW : (b + 1) * WINDOW, 0:qc] = jnp.concatenate(
+            [got[g * WINDOW : (g + 1) * WINDOW] for g in range(group)], axis=1
+        )
+
+    def pool():
+        length = rows + 2 * RIM
+        e = chan[...].astype(f32)
+        p = lax.broadcasted_iota(jnp.int32, (length, 1), 0) + (me * rows - RIM)
+        e = jnp.where((p >= 0) & (p < seq_len), e, 0.0)
+        sums = e + pltpu.roll(e, 1, 0)
+        pick = sums
+        for level in range(1, POOL_GROUPS):
+            step = 2 ** (level - 1)
+            sums = pltpu.roll(sums, step, 0) + pltpu.roll(sums, length - step, 0)
+            pick = jnp.where(t == level, sums, pick)
+        half = 1
+        for level in range(1, POOL_GROUPS):
+            half = jnp.where(t == level, 2**level, half)
+        count = (jnp.clip(p + half, 0, seq_len) - jnp.clip(p - half, 0, seq_len)).astype(f32)
+        spread = (pick[RIM : RIM + rows] / count[RIM : RIM + rows] - e[RIM : RIM + rows]).astype(bf16)
+        got = jnp.dot(spread, wp_ref[0], preferred_element_type=f32)
+        hidden[:, qc:] = (got * ps_ref[...]).astype(bf16)
+
+    def part_copy(o, src):
+        s = lax.rem(o, per)
+        owner = o // per
+        return rdma(
+            part.at[o], landed.at[src, s], part_send.at[o], part_recv.at[src, s], me, owner
+        )
+
+    def emit(i):
+        o = origin[i]
+        got = jnp.dot(hidden[:, 0:qc], wout[o, 0], preferred_element_type=f32)
+        got = got + jnp.dot(hidden[:, qc:], wout[o, 1], preferred_element_type=f32)
+        part[o] = got.astype(bf16)
+
+        @pl.when(o // per != t)
+        def _():
+            part_copy(o, t).start()
+
+    blocks = rows // WINDOW
+    relay(w_out, 0, None)
+    for b in range(1, blocks - 1):
+        attend(b)
+    relay(w_out, 1, None)
+    for c in rims:
+        c.wait()
+    pool()
+    relay(w_out, 2, None)
+    attend(0)
+    relay(w_out, 3, None)
+    attend(blocks - 1)
+    for i in range(0, 5):
+        emit(i)
+    for k in range(4, last + 1):
+        relay(w_out, k, None)
+        if k % 2 == 1:
+            emit(k)
+            emit(k + 1)
+    emit(n - 1)
+
+    share = []
+    for s in range(per):
+        total = part[t * per + s].astype(f32)
+        for j in range(1, tp):
+            src = lax.rem(t + j, tp)
+            rdma(
+                landed.at[src, s], landed.at[src, s], part_send.at[t * per + s], part_recv.at[src, s], me, src
+            ).wait_recv()
+            total = total + landed[src, s].astype(f32)
+        share.append(total)
+    mix = jnp.concatenate(share, axis=1)
+    acc[:, 0 : mix.shape[1]] = mix
+    one = jnp.sum(mix, axis=1, keepdims=True)
+    two = jnp.sum(mix * mix, axis=1, keepdims=True)
+    lane = lax.broadcasted_iota(jnp.int32, (rows, 128), 1)
+    both = jnp.where(lane == 0, one, jnp.where(lane == 1, two, 0.0))
+    stats[t] = jnp.transpose(both)[0:8]
+
+    def stat_copy(j):
+        return rdma(stats.at[t], stats.at[t], stat_send.at[j], stat_recv.at[t], me, lax.rem(t + j, tp))
+
+    for j in range(1, tp):
+        stat_copy(j).start()
+    for o in range(n):
+
+        @pl.when(o // per != t)
+        def _():
+            part_copy(o, t).wait_send()
+
+    for k in range(last + 1):
+        for way in range(2):
+            w_in(way, k, 0).wait_send()
+            w_out(way, k, 0).wait_send()
+    for b in range(per):
+        tok_copy(t, b, b, across).wait_send()
+        tok_copy(t, b, per + b, mate).wait_send()
+        tok_copy(across, b, 2 * per + b, mate).wait_send()
+    for j in range(1, tp):
+        src = lax.rem(t + j, tp)
+        rdma(stats.at[src], stats.at[src], stat_send.at[j], stat_recv.at[src], me, src).wait_recv()
+    totals = stats[0]
+    for i in range(1, tp):
+        totals = totals + stats[i]
+    wide = jnp.concatenate([totals, jnp.zeros((120, rows), f32)], axis=0)
+    back = jnp.transpose(wide)
+    width = gain_ref.shape[1] * tp
+    row_mean = back[:, 0:1] / width
+    variance = back[:, 1:2] / width - row_mean * row_mean
+    scale = lax.rsqrt(variance + epsilon)
+    out_ref[...] = ((acc[:, 0 : gain_ref.shape[1]] - row_mean) * scale * gain_ref[...]).astype(bf16)
+    for j in range(1, tp):
+        stat_copy(j).wait_send()
+
+
+def fused(n, tp, tokens, w_query, w_key, w_value, w_pool_in, sink, w_pool, pool_scale, w_out_attn, w_out_pool, out_gain):
+    rows, share = tokens.shape
+    depth, qc = w_query.shape
+    kc, cc = w_key.shape[1], w_pool_in.shape[1]
+    wide = w_out_attn.shape[1]
+    per = n // tp
+    bf16, f32 = jnp.bfloat16, jnp.float32
+    dma = pltpu.SemaphoreType.DMA
+    vmem = pl.BlockSpec(memory_space=pltpu.VMEM)
+    specs = [vmem] * 11
+    specs[5] = pl.BlockSpec(memory_space=pltpu.SMEM)
+    return pl.pallas_call(
+        functools.partial(mixer_kernel, n, tp),
+        out_shape=jax.ShapeDtypeStruct((rows, share), bf16),
+        in_specs=specs,
+        out_specs=vmem,
+        scratch_shapes=[
+            pltpu.VMEM((n, 2, depth // 2, qc + 2 * kc + cc), bf16),
+            pltpu.VMEM((n, 2, qc, wide), bf16),
+            pltpu.VMEM((n, rows, depth), bf16),
+            pltpu.VMEM((rows, qc + 2 * kc + cc), f32),
+            pltpu.VMEM((rows, qc), bf16),
+            pltpu.VMEM((rows + 2 * WINDOW, 2 * kc), bf16),
+            pltpu.VMEM((rows + 2 * RIM, cc), bf16),
+            pltpu.VMEM((rows, qc + cc), bf16),
+            pltpu.VMEM((n, rows, wide), bf16),
+            pltpu.VMEM((tp, per, rows, wide), bf16),
+            pltpu.VMEM((tp, 8, rows), f32),
+            dma((2, n - 1)),
+            dma((2, n - 1)),
+            dma((2, n - 1)),
+            dma((2, n - 1)),
+            dma((3 * per,)),
+            dma((3 * per,)),
+            dma((4,)),
+            dma((4,)),
+            dma((n,)),
+            dma((tp, per)),
+            dma((tp,)),
+            dma((tp,)),
+        ],
+        compiler_params=pltpu.CompilerParams(
+            collective_id=0, has_side_effects=True, vmem_limit_bytes=60 * 1024 * 1024
+        ),
+        name="mixer",
+    )(
+        tokens,
+        w_query,
+        w_key,
+        w_value,
+        w_pool_in,
+        sink.reshape(1, -1),
+        w_pool,
+        pool_scale.reshape(1, -1),
+        w_out_attn,
+        w_out_pool,
+        out_gain.reshape(1, -1),
+    )
+
+
+def fits(n, tp, tokens, w_query, w_key, w_pool, w_out_attn):
+    return (
+        tp == 4
+        and n == 2 * tp
+        and w_query.shape[0] % 32 == 0
+        and w_query.shape[1] % 128 == 0
+        and w_key.shape[1] == HEAD_DIM
+        and w_pool.shape[0] == 1
+        and w_out_attn.shape[1] % 128 == 0
+        and tokens.shape[0] >= 2 * WINDOW
+    )
+
+
+def mixed_rows(*args):
+    n, tp = lax.axis_size("sp"), lax.axis_size("tp")
+    if fits(n, tp, args[0], args[1], args[2], args[6], args[8]):
+        return fused(n, tp, *args)
+    return local(*args)
+
+
 def solution(mesh):
     return jax.shard_map(
-        local,
+        mixed_rows,
         mesh=mesh,
         in_specs=(
             P("sp", "tp"),

time: 219 us -> 79.9 us (0.36)
  waiting for transfers between devices: 103 us -> 0 us
  Pallas kernels: 0 us -> 75.5 us
  blocking collectives: 69.9 us -> 0 us
  matrix products: 13.9 us -> 0 us
  between operations: 13.4 us -> 0.01 us
  starting transfers between devices: 10.7 us -> 0 us
  other arithmetic: 7.57 us -> 0 us
  local copies, waits for them, and re-layouts: 0.91 us -> 4.11 us
    pallas_call x0 -> x1, Pallas kernels: none -> 75.5 us  [fused(): pl.pallas_call(functools.partial(mixer_kernel, n, tp), out_shape=jax.Shap...]
    all_gather x4 -> x0, waiting for transfers between devices: 70.9 us -> none  [the longest x1 43.5 us: local(): lax.all_gather(out_both, 'sp', axis=1, tiled=True)]
    all_gather x2 -> x0, blocking collectives: 64.1 us -> none  [the longest x1 32.8 us: local(): lax.all_gather(w_key, 'sp', axis=0, tiled=True)]
    reduce_scatter x1 -> x0, waiting for transfers between devices: 29.5 us -> none  [local(): lax.psum_scatter(terms.astype(jnp.bfloat16), 'tp', scatter_dimension=1, t...]
    dot_general x7 -> x0, matrix products: 13.9 us -> none  [the longest x1 4.25 us: local(): jnp.dot(hidden, lax.all_gather(out_both, 'sp', axis=1, tiled=True), prefe...]
    ppermute x4 -> x0, starting transfers between devices: 10.6 us -> none  [the longest x2 8 us: padded(): lax.ppermute(tail, axis, [(i, (i + 1) % count) for i in range(ends)])]
    psum x1 -> x0, blocking collectives: 5.76 us -> none  [local(): lax.psum((jnp.sum(share, axis=1), jnp.sum(share * share, axis=1)), 'tp')]
    unnamed x11 -> x5, local copies, waits for them, and re-layouts: 0.13 us -> 4.11 us
  transfers between devices with their start and end apart: 9 -> 0, of which waited for: 3 -> 0; matrix products, arithmetic and copies ran while one was open for 7% -> 0% of each run, Pallas kernels for 0% -> 0%
where the time goes in v1:
time: 79.9 us; the launch traced here: 79.7 us
  Pallas kernels  75.5 us (94%)
  local copies, waits for them, and re-layouts  4.11 us (5%)
    pallas_call x1, Pallas kernels, fused(): pl.pallas_call(functools.partial(mixer_kernel, n, tp), out_shape=jax.Shap...  75.5 us
    unnamed x5, local copies, waits for them, and re-layouts  4.11 us

profile of v1, /device:TPU:0, one launch (start us, length us, event | category | flops | bytes accessed | tf_op | source)
XLA Modules:
  0.0 79.7 jit_solution(10270141029074986044)
XLA Ops:
  0.0 0.0 copy-start
  0.0 1.5 %copy.12.wk_ref = bf16[256,64]{1,0:T(8,128)(2,1)} copy(bf16[256,64]{0,1:T(8,128)(2,1)} %param.13) | data formatting | bytes 65536 | tf_op args[2]
  1.5 0.0 copy-done
  1.5 0.7 copy.13.wv_ref
  2.2 75.5 %mixer.1 = bf16[512,512]{1,0:T(8,128)(2,1)} custom-call(bf16[512,512]{1,0:T(8,128)(2,1)} %tok_ref.1, bf16[256,256]{1,0:T(8,128)(2,1)} %wq_ref.1, bf16[256,64]{1,0:T(8,128)(2,1)} %copy.12.wk_ref, bf16[256,64]{1,0:T(8,128)(2,1)} %copy.13.wv_ref, bf16[256,256]{1,0:T(8,128)(2,1)} %wc_ref.1, f32[1,4]{1,0:T(1,128)} %bitcast.5, bf16[1,256,256]{2,1,0:T(8,128)(2,1)} %wp_ref.1, ...), custom_call_target="tpu_custom_call" | custom-call | tf_op jit(solution)/shard_map/mixer/pallas_call | solution.py:478
  77.8 1.9 %copy.15 = bf16[512,512]{1,0:T(8,128)(2,1)} copy(bf16[512,512]{1,0:T(8,128)(2,1)} %mixer.1) | data formatting | bytes 1048576
Async XLA Ops:
  0.0 1.5 %copy-start = (bf16[256,64]{0,1:T(8,128)(2,1)S(1)}, bf16[256,64]{0,1:T(8,128)(2,1)}, u32[]{:S(2)}) copy-start(bf16[256,64]{0,1:T(8,128)(2,1)} %param.14) | copy-start | bytes 98308

commit v2 on v1

--- a/solution.py
+++ b/solution.py
@@ -173,7 +173,9 @@
     chan,
     hidden,
     part,
+    mated,
     landed,
+    own,
     stats,
     win_send,
     win_recv,
@@ -184,7 +186,9 @@
     rim_send,
     rim_recv,
     part_send,
+    mate_recv,
     part_recv,
+    load,
     stat_send,
     stat_recv,
 ):
@@ -217,25 +221,35 @@
             device_id_type=MESH,
         )
 
-    qc, kc = wq_ref.shape[1], wk_ref.shape[1]
+    qc, kc = wq_ref.shape[1], wk_ref.shape[0]
     cc = wc_ref.shape[1]
     depth = wq_ref.shape[0]
     hd = depth // 2
-    for h in range(2):
-        r = slice(h * hd, (h + 1) * hd)
-        win[me, h, :, 0:qc] = wq_ref[r, :]
-        win[me, h, :, qc : qc + 2 * kc] = jnp.concatenate([wk_ref[r, :], wv_ref[r, :]], axis=1)
-        win[me, h, :, qc + 2 * kc :] = wc_ref[r, :]
-    for b in range(per):
-        tok[t * per + b] = tok_ref[:, b * depth : (b + 1) * depth]
-    wout[me, 0] = woa_ref[...]
-    wout[me, 1] = wop_ref[...]
-
     barrier = pltpu.get_barrier_semaphore()
     peers = [(s, t) for s in ring] + [(s, t) for s in (before, after)]
     peers += [(me, lax.rem(t + i, tp)) for i in range(1, tp)]
     for s, p in peers:
         pl.semaphore_signal(barrier, inc=1, device_id={"sp": s, "tp": p}, device_id_type=MESH)
+
+    loads = []
+
+    def fetch(src, dst):
+        copy = pltpu.make_async_copy(src, dst, load.at[len(loads)])
+        copy.start()
+        loads.append(copy)
+
+    for h in range(2):
+        fetch(wq_ref.at[pl.ds(h * hd, hd)], win.at[me, h, :, pl.ds(0, qc)])
+        fetch(wc_ref.at[pl.ds(h * hd, hd)], win.at[me, h, :, pl.ds(qc + 2 * kc, cc)])
+    for b in range(per):
+        fetch(tok_ref.at[:, pl.ds(b * depth, depth)], tok.at[t * per + b])
+    fetch(woa_ref, wout.at[me, 0])
+    fetch(wop_ref, wout.at[me, 1])
+    pair = jnp.transpose(jnp.concatenate([wk_ref[...], wv_ref[...]], axis=0).astype(f32)).astype(bf16)
+    for h in range(2):
+        win[me, h, :, qc : qc + 2 * kc] = pair[h * hd : (h + 1) * hd]
+    for copy in loads:
+        copy.wait()
     pl.semaphore_wait(barrier, len(peers))
 
     def ring_copy(buf, send, recv, way, k, hop):
@@ -372,12 +386,12 @@
         got = jnp.dot(spread, wp_ref[0], preferred_element_type=f32)
         hidden[:, qc:] = (got * ps_ref[...]).astype(bf16)
 
-    def part_copy(o, src):
+    def to_mate(o):
+        return rdma(part.at[o], mated.at[o], part_send.at[o], mate_recv.at[o], me, mate)
+
+    def to_owner(o):
         s = lax.rem(o, per)
-        owner = o // per
-        return rdma(
-            part.at[o], landed.at[src, s], part_send.at[o], part_recv.at[src, s], me, owner
-        )
+        return rdma(part.at[o], landed.at[s], part_send.at[o], part_recv.at[s], me, across)
 
     def emit(i):
         o = origin[i]
@@ -385,9 +399,23 @@
         got = got + jnp.dot(hidden[:, qc:], wout[o, 1], preferred_element_type=f32)
         part[o] = got.astype(bf16)
 
-        @pl.when(o // per != t)
+        @pl.when(lax.rem(o // per, 2) != lax.rem(t, 2))
         def _():
-            part_copy(o, t).start()
+            to_mate(o).start()
+
+    def combine(i):
+        o = origin[i]
+
+        @pl.when(o // per == t)
+        def _():
+            to_mate(o).wait_recv()
+            own[lax.rem(o, per)] = part[o].astype(f32) + mated[o].astype(f32)
+
+        @pl.when(o // per == across)
+        def _():
+            to_mate(o).wait_recv()
+            part[o] = (part[o].astype(f32) + mated[o].astype(f32)).astype(bf16)
+            to_owner(o).start()
 
     blocks = rows // WINDOW
     relay(w_out, 0, None)
@@ -403,23 +431,22 @@
     attend(blocks - 1)
     for i in range(0, 5):
         emit(i)
+    for i in range(0, 5):
+        combine(i)
     for k in range(4, last + 1):
         relay(w_out, k, None)
         if k % 2 == 1:
             emit(k)
             emit(k + 1)
+            combine(k)
+            combine(k + 1)
     emit(n - 1)
+    combine(n - 1)
 
     share = []
     for s in range(per):
-        total = part[t * per + s].astype(f32)
-        for j in range(1, tp):
-            src = lax.rem(t + j, tp)
-            rdma(
-                landed.at[src, s], landed.at[src, s], part_send.at[t * per + s], part_recv.at[src, s], me, src
-            ).wait_recv()
-            total = total + landed[src, s].astype(f32)
-        share.append(total)
+        to_owner(t * per + s).wait_recv()
+        share.append(own[s] + landed[s].astype(f32))
     mix = jnp.concatenate(share, axis=1)
     acc[:, 0 : mix.shape[1]] = mix
     one = jnp.sum(mix, axis=1, keepdims=True)
@@ -437,7 +464,7 @@
 
         @pl.when(o // per != t)
         def _():
-            part_copy(o, t).wait_send()
+            to_mate(o).wait_send()
 
     for k in range(last + 1):
         for way in range(2):
@@ -475,6 +502,8 @@
     vmem = pl.BlockSpec(memory_space=pltpu.VMEM)
     specs = [vmem] * 11
     specs[5] = pl.BlockSpec(memory_space=pltpu.SMEM)
+    for i in (0, 1, 4, 8, 9):
+        specs[i] = pl.BlockSpec(memory_space=pl.ANY)
     return pl.pallas_call(
         functools.partial(mixer_kernel, n, tp),
         out_shape=jax.ShapeDtypeStruct((rows, share), bf16),
@@ -490,7 +519,9 @@
             pltpu.VMEM((rows + 2 * RIM, cc), bf16),
             pltpu.VMEM((rows, qc + cc), bf16),
             pltpu.VMEM((n, rows, wide), bf16),
-            pltpu.VMEM((tp, per, rows, wide), bf16),
+            pltpu.VMEM((n, rows, wide), bf16),
+            pltpu.VMEM((per, rows, wide), bf16),
+            pltpu.VMEM((per, rows, wide), f32),
             pltpu.VMEM((tp, 8, rows), f32),
             dma((2, n - 1)),
             dma((2, n - 1)),
@@ -501,7 +532,9 @@
             dma((4,)),
             dma((4,)),
             dma((n,)),
-            dma((tp, per)),
+            dma((n,)),
+            dma((per,)),
+            dma((6 + per,)),
             dma((tp,)),
             dma((tp,)),
         ],
@@ -512,8 +545,8 @@
     )(
         tokens,
         w_query,
-        w_key,
-        w_value,
+        w_key.T,
+        w_value.T,
         w_pool_in,
         sink.reshape(1, -1),
         w_pool,

time: 79.9 us -> 69.3 us (0.87)
  Pallas kernels: 75.5 us -> 66.5 us
  local copies, waits for them, and re-layouts: 4.11 us -> 1.87 us
    pallas_call x1, Pallas kernels: 75.5 us -> 66.5 us  [fused(): pl.pallas_call(functools.partial(mixer_kernel, n, tp), out_shape=jax.Shap...]
    unnamed x5 -> x1, local copies, waits for them, and re-layouts: 4.11 us -> 1.87 us
where the time goes in v2:
time: 69.3 us; the launch traced here: 68.4 us
  Pallas kernels  66.5 us (96%)
  local copies, waits for them, and re-layouts  1.87 us (3%)
    pallas_call x1, Pallas kernels, fused(): pl.pallas_call(functools.partial(mixer_kernel, n, tp), out_shape=jax.Shap...  66.5 us
    unnamed x1, local copies, waits for them, and re-layouts  1.87 us

profile of v2, /device:TPU:0, one launch (start us, length us, event | category | flops | bytes accessed | tf_op | source)
XLA Modules:
  0.0 68.4 jit_solution(13605473591724609113)
XLA Ops:
  0.0 66.5 %mixer.1 = bf16[512,512]{1,0:T(8,128)(2,1)} custom-call(bf16[512,512]{1,0:T(8,128)(2,1)} %tok_ref.1, bf16[256,256]{1,0:T(8,128)(2,1)} %wq_ref.1, bf16[64,256]{1,0:T(8,128)(2,1)} %bitcast.5, bf16[64,256]{1,0:T(8,128)(2,1)} %bitcast.6, bf16[256,256]{1,0:T(8,128)(2,1)} %wc_ref.1, f32[1,4]{1,0:T(1,128)} %bitcast.9, bf16[1,256,256]{2,1,0:T(8,128)(2,1)} %wp_ref.1, ...), custom_call_target="tpu_custom_call" | custom-call | tf_op jit(solution)/shard_map/mixer/pallas_call | solution.py:507
  66.5 1.9 %copy.13 = bf16[512,512]{1,0:T(8,128)(2,1)} copy(bf16[512,512]{1,0:T(8,128)(2,1)} %mixer.1) | data formatting | bytes 1048576
